TPU v7x, 32 devices: a whole 2x2x4 slice. The times are simulated.
32 devices in a mesh: ep: 16 (over z, y, x), tp: 2 (over core).
Axes of the slice: x: 2, y: 2, z: 4, core: 2. Of those that a mesh axis runs over, the one named last changes fastest.
Arguments:
- tokens: bfloat16 [512, 1024], P(('ep', 'tp')), may hold values from -6 to 6
- lengths: int32 [512], P(('ep', 'tp')), may hold values from 1 to 1024
- cache_latent: bfloat16 [512, 1024, 256], P(('ep', 'tp')), may hold values from -700 to 700
- cache_rope: bfloat16 [512, 32, 1024], P(('ep', 'tp')), may hold values from -6 to 6
- attn_gain: bfloat16 [1024], replicated, may hold values from 0.099609375 to 1.8984375
- w_dq: bfloat16 [1024, 512], replicated, may hold values from -0.1875 to 0.1875
- q_gain: bfloat16 [512], replicated, may hold values from 0.099609375 to 1.8984375
- w_q_nope: bfloat16 [512, 1024], replicated, may hold values from -0.25 to 0.25
- w_q_rope: bfloat16 [512, 512], replicated, may hold values from -0.25 to 0.25
- w_dkv: bfloat16 [1024, 256], replicated, may hold values from -0.1875 to 0.1875
- kv_gain: bfloat16 [256], replicated, may hold values from 0.099609375 to 1.8984375
- w_krope: bfloat16 [1024, 32], replicated, may hold values from -0.1875 to 0.1875
- w_uk: bfloat16 [256, 1024], replicated, may hold values from -0.75 to 0.75
- w_uv: bfloat16 [256, 1024], replicated, may hold values from -0.375 to 0.375
- w_o: bfloat16 [1024, 1024], replicated, may hold values from -0.1875 to 0.1875
- post_gain: bfloat16 [1024], replicated, may hold values from 0.099609375 to 1.8984375
- moe_gain: bfloat16 [1024], replicated, may hold values from 0.099609375 to 1.8984375
- routes: int32 [512, 4], P(('ep', 'tp')), may hold values from 0 to 15, all different within a row; in each aligned block of 16 rows (0 to 15, 16 to 31, ...) at most 6 rows name the same one
- route_scores: float32 [512, 4], P(('ep', 'tp')), may hold values from 0.05 to 1
- expert_gate: bfloat16 [16, 1024, 512], P('ep', None, 'tp'), may hold values from -0.1875 to 0.1875
- expert_up: bfloat16 [16, 1024, 512], P('ep', None, 'tp'), may hold values from -0.1875 to 0.1875
- expert_down: bfloat16 [16, 512, 1024], P('ep', 'tp'), may hold values from -0.25 to 0.25
- shared_gate: bfloat16 [1024, 512], replicated, may hold values from -0.1875 to 0.1875
- shared_up: bfloat16 [1024, 512], replicated, may hold values from -0.1875 to 0.1875
- shared_down: bfloat16 [512, 1024], replicated, may hold values from -0.25 to 0.25
- dense_vec: bfloat16 [1024], replicated, may hold values from -0.1875 to 0.1875
- dense_w_gate: bfloat16 [1024, 8192], P(None, ('ep', 'tp')), may hold values from -0.1875 to 0.1875
- dense_w_up: bfloat16 [1024, 8192], P(None, ('ep', 'tp')), may hold values from -0.1875 to 0.1875
- dense_w_down: bfloat16 [8192, 1024], P(('ep', 'tp')), may hold values from -0.125 to 0.125
- out_gain: bfloat16 [1024], replicated, may hold values from 0.099609375 to 1.8984375
Outputs:
- hidden_out: bfloat16 [512, 1024], P(('ep', 'tp'))
- new_latent: bfloat16 [512, 256], P(('ep', 'tp'))
Inputs may be any that keep to these rules, and one draw needn't show every extreme that they name: `routes`: each row names 4 different experts. In the 16 rows of one device no expert is named more than 6 times, a bound that some block reaches in some devices' rows.
All inputs are finite; a program needn't handle non-finite values.
Results may differ from a plain program's by a relative error of at most 0.011.
The roundings to bfloat16 on the way count: a program that leaves them out, or rounds other values in their place, can miss the bound.
Values may be sent and summed in bfloat16 or wider, within the bound.
A program may use at most 128 MiB of HBM per device.

v0:
```python
import functools

import jax
import jax.numpy as jnp
from jax import lax
from jax.experimental import pallas as pl
from jax.experimental.pallas import tpu as pltpu
from jax.sharding import PartitionSpec as P

HEADS = 16
NOPE = 64
ROPE = 32
VDIM = 64


eps = 1e-06
rope_base = 10000.0
routed_scale = 2.5


def rms_scale(value, gain):
    value = value.astype(jnp.float32)
    inverse = lax.rsqrt(jnp.mean(value * value, axis=-1, keepdims=True) + eps)
    return value * inverse * gain.astype(jnp.float32)


def angles(lengths, rope_dim):
    half = rope_dim // 2
    freqs = rope_base ** (-jnp.arange(half, dtype=jnp.float32) / half)
    angle = lengths.astype(jnp.float32)[:, None] * freqs[None, :]
    return (jnp.cos(angle), jnp.sin(angle))


def attention_kernel(
    batch,
    experts,
    lens_ref,
    tokens_ref,
    cos_ref,
    sin_ref,
    routes_ref,
    scores_ref,
    attn_gain,
    q_gain,
    kv_gain,
    post_gain,
    moe_gain,
    dense_vec,
    *refs,
):
    f32, bf16 = jnp.float32, jnp.bfloat16
    hbm, (first_ref, x_ref, latent_out), bufs = refs[:10], refs[10:13], refs[13:23]
    query, spun, mixed, sem, cache_sem = refs[23:]
    w_dq, w_dkv, w_krope, w_q_nope, w_q_rope, w_uk, latent, rope, w_uv, w_o = bufs
    seqs, length, wide = latent.shape
    width = tokens_ref.shape[1]

    weights = [0, 1, 2, 3, 4, 5, 8, 9]
    loads = {i: pltpu.make_async_copy(hbm[i], bufs[i], sem.at[i]) for i in weights}

    def cache_load(s):
        return (
            pltpu.make_async_copy(hbm[6].at[s], latent.at[s], cache_sem.at[0, s]),
            pltpu.make_async_copy(hbm[7].at[s], rope.at[s], cache_sem.at[1, s]),
        )

    for i in weights[:6]:
        loads[i].start()

    @pl.loop(0, seqs)
    def _(s):
        for load in cache_load(s):
            load.start()

    for i in weights[6:]:
        loads[i].start()

    def mul(a, b):
        return jnp.dot(a, b, preferred_element_type=f32)

    def mul_t(a, b):
        return lax.dot_general(a, b, (((1,), (1,)), ((), ())), preferred_element_type=f32)

    tokens = tokens_ref[...].astype(f32)
    normed = rms_scale(tokens, attn_gain[...][None, :]).astype(bf16)
    loads[0].wait()
    q_normed = rms_scale(mul(normed, w_dq[...]), q_gain[...][None, :]).astype(bf16)
    loads[1].wait()
    new_latent = rms_scale(mul(normed, w_dkv[...]), kv_gain[...][None, :]).astype(bf16)
    latent_out[...] = new_latent
    fresh = new_latent.astype(f32)
    loads[2].wait()
    half = ROPE // 2
    raw = mul_t(normed, w_krope[...])
    swapped = jnp.concatenate([raw[:, half:], raw[:, :half]], axis=1)
    new_rope = (raw * cos_ref[:, :ROPE] + swapped * sin_ref[:, :ROPE]).astype(bf16).astype(f32)
    loads[3].wait()
    q_nope = mul(q_normed, w_q_nope[...]).astype(bf16)
    loads[4].wait()
    raw = mul(q_normed, w_q_rope[...])
    span = raw.shape[1]
    lane = lax.broadcasted_iota(jnp.int32, raw.shape, 1)
    swapped = jnp.where(
        lane % ROPE < half, pltpu.roll(raw, span - half, 1), pltpu.roll(raw, half, 1)
    )
    q_rot = (raw * cos_ref[...] + swapped * sin_ref[...]).astype(bf16).astype(f32)
    for h in range(HEADS):
        spun[:, h, :] = q_rot[:, h * ROPE : (h + 1) * ROPE]
    loads[5].wait()
    low = lax.broadcasted_iota(jnp.int32, (seqs, 2 * NOPE), 1) < NOPE
    for pair in range(HEADS // 2):
        at = slice(pair * 2 * NOPE, (pair + 1) * 2 * NOPE)
        both = q_nope[:, at].astype(f32)
        both = jnp.concatenate([jnp.where(low, both, 0.0), jnp.where(low, 0.0, both)], axis=0)
        lat = mul_t(both.astype(bf16), w_uk[:, at]).astype(bf16).astype(f32)
        query[:, 2 * pair, :] = lat[:seqs]
        query[:, 2 * pair + 1, :] = lat[seqs:]

    scale = (NOPE + ROPE) ** (-0.5)
    place = lax.broadcasted_iota(jnp.int32, (HEADS, length), 1)
    row = lax.broadcasted_iota(jnp.int32, (seqs, 1), 0)

    @pl.loop(0, seqs // batch)
    def _(step):
        ids = [step * batch + i for i in range(batch)]
        for s in ids:
            for load in cache_load(s):
                load.wait()
        for s in ids:
            mine, turned, keys = query[s], spun[s], latent[s]
            own_key = jnp.sum(jnp.where(row == s, fresh, 0.0), axis=0, keepdims=True)
            own_rope = jnp.sum(jnp.where(row == s, new_rope, 0.0), axis=0, keepdims=True)
            past = (mul_t(mine.astype(bf16), keys) + mul(turned.astype(bf16), rope[s])) * scale
            own = jnp.sum(mine * own_key, axis=1, keepdims=True)
            own = (own + jnp.sum(turned * own_rope, axis=1, keepdims=True)) * scale
            valid = place < lens_ref[s]
            top = jnp.max(jnp.where(valid, past, -1e30), axis=1, keepdims=True)
            top = jnp.maximum(top, own)
            past = jnp.where(valid, jnp.exp(past - top), 0.0)
            own = jnp.exp(own - top)
            total = jnp.sum(past, axis=1, keepdims=True) + own
            out = mul((past / total).astype(bf16), keys)
            mixed[s] = out + (own / total).astype(bf16).astype(f32) * own_key

    loads[8].wait()
    parts = []
    for pair in range(HEADS // 2):
        at = slice(pair * 2 * VDIM, (pair + 1) * 2 * VDIM)
        both = jnp.concatenate([mixed[:, 2 * pair, :], mixed[:, 2 * pair + 1, :]], axis=0)
        both = mul(both.astype(bf16), w_uv[:, at])
        lane = lax.broadcasted_iota(jnp.int32, (seqs, 2 * VDIM), 1)
        parts.append(jnp.where(lane < VDIM, both[:seqs], both[seqs:]))
    head_out = jnp.concatenate(parts, axis=1).astype(bf16)
    loads[9].wait()
    first = (tokens + rms_scale(mul(head_out, w_o[...]), post_gain[...][None, :])).astype(bf16)
    first_ref[...] = first
    moe_in = rms_scale(first, moe_gain[...][None, :]).astype(bf16)
    x_ref[:, :width] = moe_in
    gate = jnp.sum(moe_in.astype(f32) * dense_vec[...][None, :].astype(f32), axis=1, keepdims=True)
    gate = jax.nn.sigmoid(gate)
    columns = experts + 1
    lane = lax.broadcasted_iota(jnp.int32, (seqs, x_ref.shape[1] - width), 1)
    routes, scores = routes_ref[...], scores_ref[...]
    norm = scores / jnp.sum(scores, axis=1, keepdims=True) * routed_scale
    rest = jnp.where(lane % columns == experts, gate, 0.0)
    for t in range(routes.shape[1]):
        rest = rest + jnp.where(lane % columns == routes[:, t : t + 1], norm[:, t : t + 1], 0.0)
    out = jnp.zeros_like(rest)
    for part in range(PARTS):
        piece = rest.astype(bf16).astype(f32)
        here = (lane >= part * columns) & (lane < (part + 1) * columns)
        out = jnp.where(here, piece, out)
        rest = rest - piece
    x_ref[:, width:] = out.astype(bf16)


def attention(tokens, lengths, routes, scores, experts, gains, big):
    f32, bf16 = jnp.float32, jnp.bfloat16
    seqs, width = tokens.shape
    cosine, sine = angles(lengths, ROPE)
    cosine = jnp.tile(jnp.concatenate([cosine, cosine], axis=1), (1, HEADS))
    sine = jnp.tile(jnp.concatenate([-sine, sine], axis=1), (1, HEADS))
    wide = big[6].shape[2]
    batch = 4 if seqs % 4 == 0 else 1
    vmem = pl.BlockSpec(memory_space=pltpu.VMEM)
    return pl.pallas_call(
        functools.partial(attention_kernel, batch, experts),
        out_shape=(
            jax.ShapeDtypeStruct((seqs, width), bf16),
            jax.ShapeDtypeStruct((seqs, width + meta_width(experts)), bf16),
            jax.ShapeDtypeStruct((seqs, wide), bf16),
        ),
        in_specs=[pl.BlockSpec(memory_space=pltpu.SMEM)]
        + [vmem] * 11
        + [pl.BlockSpec(memory_space=pltpu.HBM)] * 10,
        out_specs=(vmem, vmem, vmem),
        scratch_shapes=[pltpu.VMEM(w.shape, w.dtype) for w in big]
        + [
            pltpu.VMEM((seqs, HEADS, wide), f32),
            pltpu.VMEM((seqs, HEADS, ROPE), f32),
            pltpu.VMEM((seqs, HEADS, wide), f32),
            pltpu.SemaphoreType.DMA((10,)),
            pltpu.SemaphoreType.DMA((2, seqs)),
        ],

        name="attention",
    )(lengths, tokens, cosine, sine, routes, scores, *gains, *big)


MESH = pl.DeviceIdType.MESH
PARTS = 3


def partner(me, k, count):
    other, bit = me, 1
    while bit < count:
        other = other + bit * ((k // bit) % 2) * (1 - 2 * ((me // bit) % 2))
        bit *= 2
    return other


def meta_width(experts):
    return -(-PARTS * (experts + 1) // 128) * 128


def exchange_kernel(
    count,
    groups,
    x_ref,
    first_ref,
    gain_ref,
    eg_hbm,
    eu_hbm,
    ed_hbm,
    dg_hbm,
    du_hbm,
    dd_hbm,
    sg_hbm,
    su_hbm,
    sd_hbm,
    out_ref,
    eg,
    eu,
    ed,
    dg,
    du,
    dd,
    sg,
    su,
    sd,
    rows,
    keep,
    to_sib,
    from_sib,
    to_home,
    from_home,
    load_sem,
    row_send,
    row_recv,
    relay_send,
    relay_recv,
    sib_send,
    sib_recv,
    home_send,
    home_recv,
):
    f32, bf16 = jnp.float32, jnp.bfloat16
    seqs, wide = x_ref.shape
    width = first_ref.shape[1]
    me = lax.axis_index("ep")
    core = lax.axis_index("tp")
    sibling = (me, 1 - core)
    size = count // groups

    loads = [
        pltpu.make_async_copy(src, dst, load_sem.at[i])
        for i, (src, dst) in enumerate(
            (
                (sg_hbm, sg),
                (su_hbm, su),
                (sd_hbm, sd),
                (eg_hbm.at[0], eg),
                (eu_hbm.at[0], eu),
                (dg_hbm, dg),
                (du_hbm, du),
                (ed_hbm.at[0], ed),
                (dd_hbm, dd),
            )
        )
    ]
    for load in loads:
        load.start()

    barrier = pltpu.get_barrier_semaphore()
    pl.semaphore_signal(barrier, inc=1, device_id=sibling, device_id_type=MESH)

    @pl.loop(1, count)
    def _(k):
        pl.semaphore_signal(
            barrier, inc=1, device_id=(partner(me, k, count), core), device_id_type=MESH
        )

    pl.semaphore_wait(barrier, count)

    def row_copy(k, src, hop):
        return pltpu.make_async_remote_copy(
            src_ref=src,
            dst_ref=rows.at[0, k],
            send_sem=row_send.at[k],
            recv_sem=row_recv.at[k],
            device_id=(partner(me, hop, count), core),
            device_id_type=MESH,
        )

    def relay_copy(k, src):
        return pltpu.make_async_remote_copy(
            src_ref=src,
            dst_ref=rows.at[1, k],
            send_sem=relay_send.at[k],
            recv_sem=relay_recv.at[k],
            device_id=sibling,
            device_id_type=MESH,
        )

    def sib_copy(g):
        return pltpu.make_async_remote_copy(
            src_ref=to_sib.at[pl.ds(g * size, size)],
            dst_ref=from_sib.at[pl.ds(g * size, size)],
            send_sem=sib_send.at[g],
            recv_sem=sib_recv.at[g],
            device_id=sibling,
            device_id_type=MESH,
        )

    def home_copy(k, hop):
        return pltpu.make_async_remote_copy(
            src_ref=to_home.at[k],
            dst_ref=from_home.at[k],
            send_sem=home_send.at[k],
            recv_sem=home_recv.at[k],
            device_id=(partner(me, hop, count), core),
            device_id_type=MESH,
        )

    for g in range(1, groups):
        row_copy(g * size, x_ref, g * size).start()

    @pl.loop(1, size)
    def _(m):
        row_copy(m, x_ref, m).start()

    relay_copy(0, x_ref).start()
    own = pltpu.make_async_copy(x_ref, rows.at[0, 0], row_recv.at[0])
    own.start()

    for load in loads[:3]:
        load.wait()
    mine = x_ref[:, :width]
    hidden = (
        jax.nn.silu(jnp.dot(mine, sg[...], preferred_element_type=f32))
        * jnp.dot(mine, su[...], preferred_element_type=f32)
    ).astype(bf16)
    total = jnp.dot(hidden, sd[...], preferred_element_type=f32)
    for g in range(1, groups):
        row_copy(g * size, x_ref, g * size).wait_recv()

        @pl.loop(1, size)
        def _(m):
            row_copy(g * size + m, rows.at[0, g * size], m).start()

    for load in loads[3:]:
        load.wait()
    own.wait()

    lane = lax.broadcasted_iota(jnp.int32, (1, wide - width), 1)
    columns = count + 1

    def picked(meta, column):
        chosen = lane == column
        for part in range(1, PARTS):
            chosen = chosen | (lane == column + part * columns)
        return jnp.sum(jnp.where(chosen, meta, 0.0), axis=1, keepdims=True)

    def send_home(g):
        sib_copy(g).wait_recv()
        part = keep[g * size : (g + 1) * size] + from_sib[g * size : (g + 1) * size].astype(f32)
        to_home[g * size : (g + 1) * size] = part.astype(bf16)

        keep[g * size] = part[0]

        @pl.loop(1, size)
        def _(m):
            home_copy(g * size + m, m).start()

    def plane_sum(g):
        @pl.loop(1, size)
        def _(m):
            home_copy(g * size + m, m).wait_recv()

        part = keep[g * size]
        for m in range(1, size):
            part = part + from_home[g * size + m].astype(f32)
        return part

    def send_far(g):
        to_home[g * size] = plane_sum(g).astype(bf16)
        home_copy(g * size, g * size).start()

    order = list(range(1, groups)) + [0]
    for turn, g in enumerate(order):
        if g > 0:
            relay_copy(g * size, rows.at[0, g * size]).start()

        @pl.loop(g * size + 1, (g + 1) * size)
        def _(k):
            row_copy(k, x_ref, 1).wait_recv()
            relay_copy(k, rows.at[0, k]).start()

        if turn > 0:
            send_home(order[turn - 1])

        @pl.loop(g * size, (g + 1) * size)
        def _(k):
            relay_copy(k, x_ref).wait_recv()

        block = rows[:, g * size : (g + 1) * size].reshape(2 * size * seqs, wide)
        values, meta = block[:, :width], block[:, width:].astype(f32)
        act = (
            jax.nn.silu(jnp.dot(values, eg[...], preferred_element_type=f32))
            * jnp.dot(values, eu[...], preferred_element_type=f32)
        ).astype(bf16)
        routed = jnp.dot(act, ed[...], preferred_element_type=f32).astype(bf16).astype(f32)
        act = (
            jax.nn.silu(jnp.dot(values, dg[...], preferred_element_type=f32))
            * jnp.dot(values, du[...], preferred_element_type=f32)
        ).astype(bf16)
        dense = jnp.dot(act, dd[...], preferred_element_type=f32)
        part = routed * picked(meta, me) + dense * picked(meta, count)
        part = part.reshape(2, size, seqs, width)
        to_sib[g * size : (g + 1) * size] = part[1].astype(bf16)
        sib_copy(g).start()
        keep[g * size : (g + 1) * size] = part[0]

    send_home(order[-1])
    for g in range(1, groups):
        send_far(g)
    total = total + plane_sum(0)
    for g in range(1, groups):
        home_copy(g * size, g * size).wait_recv()
        total = total + from_home[g * size].astype(f32)
    inverse = lax.rsqrt(jnp.mean(total * total, axis=-1, keepdims=True) + eps)
    out_ref[...] = (
        first_ref[...].astype(f32) + total * inverse * gain_ref[...][None, :].astype(f32)
    ).astype(bf16)

    relay_copy(0, x_ref).wait_send()

    @pl.loop(1, count)
    def _(k):
        row_copy(k, x_ref, 1).wait_send()
        relay_copy(k, rows.at[0, k]).wait_send()
        home_copy(k, 1).wait_send()

    for g in range(groups):
        sib_copy(g).wait_send()


def exchange(rows, first, gain, expert, dense, shared):
    bf16, f32 = jnp.bfloat16, jnp.float32
    count = lax.axis_size("ep")
    groups = min(4, count)
    seqs, width = first.shape
    wide = rows.shape[1]
    any_space = pl.BlockSpec(memory_space=pltpu.HBM)
    vmem = pl.BlockSpec(memory_space=pltpu.VMEM)
    dma = pltpu.SemaphoreType.DMA
    weights = list(expert) + list(dense) + list(shared)
    return pl.pallas_call(
        functools.partial(exchange_kernel, count, groups),
        out_shape=jax.ShapeDtypeStruct((seqs, width), bf16),
        in_specs=[vmem] * 3 + [any_space] * 9,
        out_specs=vmem,
        scratch_shapes=[pltpu.VMEM(w.shape[-2:], w.dtype) for w in weights]
        + [
            pltpu.VMEM((2, count, seqs, wide), bf16),
            pltpu.VMEM((count, seqs, width), f32),
            pltpu.VMEM((count, seqs, width), bf16),
            pltpu.VMEM((count, seqs, width), bf16),
            pltpu.VMEM((count, seqs, width), bf16),
            pltpu.VMEM((count, seqs, width), bf16),
            dma((9,)),
            dma((count,)),
            dma((count,)),
            dma((count,)),
            dma((count,)),
            dma((groups,)),
            dma((groups,)),
            dma((count,)),
            dma((count,)),
        ],
        compiler_params=pltpu.CompilerParams(
            collective_id=0, has_side_effects=True
        ),
        name="exchange",
    )(rows, first, gain, *weights)


def shards(
    tokens,
    lengths,
    cache_latent,
    cache_rope,
    attn_gain,
    w_dq,
    q_gain,
    w_q_nope,
    w_q_rope,
    w_dkv,
    kv_gain,
    w_krope,
    w_uk,
    w_uv,
    w_o,
    post_gain,
    moe_gain,
    routes,
    route_scores,
    expert_gate,
    expert_up,
    expert_down,
    shared_gate,
    shared_up,
    shared_down,
    dense_vec,
    dense_w_gate,
    dense_w_up,
    dense_w_down,
    out_gain,
):
    experts = expert_gate.shape[0] * lax.axis_size("ep")
    first, rows, new_latent = attention(
        tokens,
        lengths,
        routes,
        route_scores,
        experts,
        (attn_gain, q_gain, kv_gain, post_gain, moe_gain, dense_vec),
        (w_dq, w_dkv, w_krope.T, w_q_nope, w_q_rope, w_uk, cache_latent, cache_rope, w_uv, w_o),
    )
    hidden_out = exchange(
        rows,
        first,
        out_gain,
        (expert_gate, expert_up, expert_down),
        (dense_w_gate, dense_w_up, dense_w_down),
        (shared_gate, shared_up, shared_down),
    )
    return (hidden_out, new_latent)


def solution(mesh):
    return jax.shard_map(
        shards,
        mesh=mesh,
        in_specs=(
            P(("ep", "tp"), None),
            P(("ep", "tp")),
            P(("ep", "tp"), None, None),
            P(("ep", "tp"), None, None),
            P(),
            P(),
            P(),
            P(),
            P(),
            P(),
            P(),
            P(),
            P(),
            P(),
            P(),
            P(),
            P(),
            P(("ep", "tp"), None),
            P(("ep", "tp"), None),
            P("ep", None, "tp"),
            P("ep", None, "tp"),
            P("ep", "tp", None),
            P(),
            P(),
            P(),
            P(),
            P(None, ("ep", "tp")),
            P(None, ("ep", "tp")),
            P(("ep", "tp"), None),
            P(),
        ),
        out_specs=(P(("ep", "tp"), None), P(("ep", "tp"), None)),
        check_vma=False,
    )
```

profile of v0, /device:TPU:0, one launch (start us, length us, event | category | flops | bytes accessed | tf_op | source)
XLA Modules:
  0.0 53.3 jit_solution(6453117170824348747)
XLA Ops:
  0.6 0.7 %convert_element_type.3 = f32[16]{0:T(128)S(1)} convert(s32[16]{0:T(128)} %lens_ref.1) | non-fusion elementwise | flops 16 | bytes 128 | tf_op jit(solution)/shard_map/convert_element_type | solution.py:30
  1.3 0.1 fusion
  1.4 0.1 pad_maximum_fusion
  1.5 0.7 %tile.21.sin_ref = f32[16,512]{1,0:T(8,128)} reshape(f32[16,16,32]{2,1,0:T(8,128)S(1)} %tile.20) | data formatting | bytes 65536 | tf_op jit(solution)/shard_map/tile | solution.py:182
  2.2 0.7 %tile.9.cos_ref = f32[16,512]{1,0:T(8,128)} reshape(f32[16,16,32]{2,1,0:T(8,128)S(1)} %tile.8) | data formatting | bytes 65536 | tf_op jit(solution)/shard_map/tile | solution.py:181
  3.0 1.4 %copy.32.routes_ref = s32[16,4]{1,0:T(8,128)} copy(s32[16,4]{0,1:T(4,128)} %param.47) | data formatting | bytes 512 | tf_op args[17]
  4.3 1.3 %copy.33.scores_ref = f32[16,4]{1,0:T(8,128)} copy(f32[16,4]{0,1:T(4,128)} %param.48) | data formatting | bytes 512 | tf_op args[18]
  5.7 15.6 %attention.1 = (bf16[16,1024]{1,0:T(8,128)(2,1)}, bf16[16,1152]{1,0:T(8,128)(2,1)}, bf16[16,256]{1,0:T(8,128)(2,1)}) custom-call(s32[16]{0:T(128)} %lens_ref.1, bf16[16,1024]{1,0:T(8,128)(2,1)} %tokens_ref.1, f32[16,512]{1,0:T(8,128)} %tile.9.cos_ref, f32[16,512]{1,0:T(8,128)} %tile.21.sin_ref, s32[16,4]{1,0:T(8,128)} %copy.32.routes_ref, ...), custom_call_target="tpu_custom_call" | custom-call | tf_op jit(solution)/shard_map/attention/pallas_call | solution.py:186
  21.2 30.7 %exchange.1 = bf16[16,1024]{1,0:T(8,128)(2,1)} custom-call(bf16[16,1152]{1,0:T(8,128)(2,1)} %get-tuple-element.5.x_ref, bf16[16,1024]{1,0:T(8,128)(2,1)} %get-tuple-element.6.first_ref, bf16[1024]{0:T(1024)(128)(2,1)} %gain_ref.1, bf16[1,1024,256]{2,1,0:T(8,128)(2,1)} %eg_hbm.1, bf16[1,1024,256]{2,1,0:T(8,128)(2,1)} %eu_hbm.1, bf16[1,256,1024]{2,1,0:T(8,128)(2,1)} %ed_hbm.1, ...), custom_call_target="tpu_custom_call" | custom-call | tf_op jit(solution)/shard_map/exchange/pallas_call | solution.py:478
  51.9 1.4 %copy.35 = bf16[16,1024]{1,0:T(8,128)(2,1)} copy(bf16[16,1024]{1,0:T(8,128)(2,1)} %exchange.1) | data formatting | bytes 65536
  (3 shorter events, 0.0 us)
where the time goes:
time: 53.7 us; the launch traced here: 53.3 us
  Pallas kernels  46.3 us (86%)
  local copies, waits for them, and re-layouts  5.52 us (10%)
  other arithmetic  0.87 us (2%)
  between operations  0.66 us (1%)
    pallas_call x1, Pallas kernels, exchange(): pl.pallas_call(functools.partial(exchange_kernel, count, groups), out_sha...  30.7 us
    pallas_call x1, Pallas kernels, attention(): pl.pallas_call(functools.partial(attention_kernel, batch, experts), out_s...  15.6 us
    unnamed x3, local copies, waits for them, and re-layouts  4.08 us

commit v1 on v0

v1 whole, which is shorter than its diff:
```python
import functools

import jax
import jax.numpy as jnp
from jax import lax
from jax.experimental import pallas as pl
from jax.experimental.pallas import tpu as pltpu
from jax.sharding import PartitionSpec as P

HEADS = 16
NOPE = 64
ROPE = 32
VDIM = 64


eps = 1e-06
rope_base = 10000.0
routed_scale = 2.5


def rms_scale(value, gain):
    value = value.astype(jnp.float32)
    inverse = lax.rsqrt(jnp.mean(value * value, axis=-1, keepdims=True) + eps)
    return value * inverse * gain.astype(jnp.float32)


MESH = pl.DeviceIdType.MESH


def partner(me, k, count):
    other, bit = me, 1
    while bit < count:
        if (k // bit) % 2:
            other = other + bit * (1 - 2 * ((me // bit) % 2))
        bit *= 2
    return other


def bits_of(size):
    return [1 << i for i in range(size.bit_length() - 1)]


def low_bit(m):
    return m & -m


def high_bit(m):
    return 1 << (m.bit_length() - 1)


def layer_kernel(
    count,
    groups,
    *refs,
):
    f32, bf16 = jnp.float32, jnp.bfloat16
    small, hbm, (out_ref, latent_out) = refs[:11], refs[11:30], refs[30:32]
    smalls, bufs = refs[32:43], refs[43:59]
    (query, spun, scores, probs, mixed, rows, route_out, route_in) = refs[59:67]
    (keep, to_sib, from_sib, to_home, from_home) = refs[67:72]
    (small_sem, load_sem, cache_sem, meta_sem, send_sem, row_recv, relay_recv) = refs[72:79]
    sib_recv, home_recv = refs[79:]
    (tokens_ref, lens_ref, routes_ref, scores_ref, attn_gain, q_gain, kv_gain) = smalls[:7]
    post_gain, moe_gain, dense_vec, out_gain = smalls[7:]
    w_dq, w_dkv, w_krope, w_q_nope, w_q_rope, w_uk, latent, rope, w_uv, w_o = bufs[:10]
    s_in, s_down, e_in, e_down, d_in, d_down = bufs[10:]
    seqs, width = tokens_ref.shape
    batches, length, spread = latent.shape
    batch = seqs // batches
    wide = spread // batch
    tall = HEADS * batch
    size = count // groups
    half_width = width // 2
    me = lax.axis_index("ep")
    core = lax.axis_index("tp")
    sibling = (me, 1 - core)

    def peer(k):
        return (partner(me, k, count), core)

    small_loads = [
        pltpu.make_async_copy(src, dst, small_sem.at[i])
        for i, (src, dst) in enumerate(zip(small, smalls))
    ]
    for load in small_loads:
        load.start()

    def wait_small(*ids):
        for i in ids:
            small_loads[i].wait()

    loads = {
        i: pltpu.make_async_copy(hbm[i], bufs[i], load_sem.at[i])
        for i in (0, 1, 2, 3, 4, 5, 8, 9)
    }
    stacked = [
        (hbm[10], s_in.at[0], 10),
        (hbm[11], s_in.at[1], 10),
        (hbm[12], s_down, 11),
        (hbm[13].at[0], e_in.at[0], 12),
        (hbm[14].at[0], e_in.at[1], 12),
        (hbm[17].at[0], e_down, 13),
        (hbm[15], d_in.at[0], 6),
        (hbm[16], d_in.at[1], 6),
        (hbm[18], d_down, 7),
    ]

    def whole(ref, sem):
        return pltpu.make_async_copy(ref, ref, sem)

    def load_cache(b):
        for j in range(batch):
            s = b * batch + j
            dst = latent.at[b, :, pl.ds(j * wide, wide)]
            pltpu.make_async_copy(hbm[6].at[s], dst, cache_sem.at[0, b]).start()
            pltpu.make_async_copy(hbm[7].at[s], rope.at[b, j], cache_sem.at[1, b]).start()

    for i in range(3):
        loads[i].start()

    barrier = pltpu.get_barrier_semaphore()
    pl.semaphore_signal(barrier, inc=1, device_id=sibling, device_id_type=MESH)
    for k in range(1, count):
        other = partner(me, k, count)
        for c in (core, 1 - core):
            pl.semaphore_signal(barrier, inc=1, device_id=(other, c), device_id_type=MESH)

    def mul(a, b):
        return jnp.dot(a, b, preferred_element_type=f32)

    def mul_t(a, b):
        return lax.dot_general(a, b, (((1,), (1,)), ((), ())), preferred_element_type=f32)

    line = lax.broadcasted_iota(jnp.int32, (seqs, 128), 0)
    lane = lax.broadcasted_iota(jnp.int32, (seqs, 128), 1)

    def upright(flat):
        wide_line = lax.broadcasted_iota(jnp.int32, (seqs, seqs), 0)
        wide_lane = lax.broadcasted_iota(jnp.int32, (seqs, seqs), 1)
        return jnp.sum(jnp.where(wide_line == wide_lane, flat, 0.0), axis=1, keepdims=True)

    wait_small(2, 3)
    for i in range(3, 6):
        loads[i].start()
    share = scores_ref[...] / jnp.sum(scores_ref[...], axis=0, keepdims=True) * routed_scale
    routes = routes_ref[...]
    experts = route_out.shape[0]
    expert = lax.broadcasted_iota(jnp.int32, (experts, seqs), 0)
    table = jnp.zeros((experts, seqs), f32)
    for t in range(routes.shape[0]):
        table = table + jnp.where(expert == routes[t : t + 1], share[t : t + 1], 0.0)
    table = jnp.concatenate([table, jnp.zeros((experts, 128 - seqs), f32)], axis=1)
    for e in range(experts):
        route_out[e] = table[e : e + 1]

    wait_small(1)
    lens = jnp.broadcast_to(upright(lens_ref[...][None, :].astype(f32)), (seqs, 128))
    half = ROPE // 2
    freq = jnp.zeros((seqs, 128), f32)
    for i in range(half):
        freq = jnp.where(lane % half == i, float(rope_base ** (-i / half)), freq)
    angle = lens * freq
    cosine = jnp.cos(angle)
    sine = jnp.sin(angle)
    sine = jnp.where(lane % ROPE < half, -sine, sine)

    def spin(raw):
        swapped = jnp.where(
            lane % ROPE < half, pltpu.roll(raw, 128 - half, 1), pltpu.roll(raw, half, 1)
        )
        return (raw * cosine + swapped * sine).astype(bf16).astype(f32)

    wait_small(0, 4)
    tokens = tokens_ref[...].astype(f32)
    normed = rms_scale(tokens, attn_gain[...][None, :]).astype(bf16)
    wait_small(5, 6)
    loads[0].wait()
    load_cache(0)
    q_normed = rms_scale(mul(normed, w_dq[...]), q_gain[...][None, :]).astype(bf16)
    loads[1].wait()
    new_latent = rms_scale(mul(normed, w_dkv[...]), kv_gain[...][None, :]).astype(bf16)
    latent_out[...] = new_latent
    fresh = new_latent.astype(f32)
    loads[2].wait()
    raw = mul_t(normed, w_krope[...])
    new_rope = spin(jnp.concatenate([raw] * (128 // ROPE), axis=1))
    loads[3].wait()
    q_nope = mul(q_normed, w_q_nope[...]).astype(bf16)
    loads[4].wait()
    raw = mul(q_normed, w_q_rope[...])
    per = 128 // ROPE
    for a in range(HEADS // per):
        turned = spin(raw[:, a * 128 : (a + 1) * 128])
        rolled = [turned] + [pltpu.roll(turned, d * ROPE, 1) for d in range(1, per)]
        for j in range(per):
            pick = rolled[0]
            for d in range(1, per):
                pick = jnp.where((line - j) % per == d, rolled[d], pick)
            pick = jnp.where(lane // ROPE == line % per, pick, 0.0)
            h = a * per + j
            for b in range(batches):
                for v in range(batch // per):
                    spun[b, h * batch : (h + 1) * batch, v * 128 : (v + 1) * 128] = jnp.where(
                        (line % batch) // per == v, pick, 0.0
                    )[b * batch : (b + 1) * batch]
    loads[5].wait()
    for i in range(1, batches):
        load_cache(i)
    loads[8].start()
    loads[9].start()
    low = lax.broadcasted_iota(jnp.int32, (seqs, 2 * NOPE), 1) < NOPE
    for pair in range(HEADS // 2):
        at = slice(pair * 2 * NOPE, (pair + 1) * 2 * NOPE)
        both = q_nope[:, at].astype(f32)
        both = jnp.concatenate([jnp.where(low, both, 0.0), jnp.where(low, 0.0, both)], axis=0)
        lat = mul_t(both.astype(bf16), w_uk[:, at]).astype(bf16).astype(f32)
        for i in range(2):
            for b in range(batches):
                h = 2 * pair + i
                query[b, h * batch : (h + 1) * batch, :] = lat[
                    i * seqs + b * batch : i * seqs + (b + 1) * batch
                ]

    pl.semaphore_wait(barrier, 2 * count - 1)

    others = [(c, k) for c in range(2) for k in range(count) if c + k > 0]
    for c, k in others:
        other = partner(me, k, count)
        pltpu.make_async_remote_copy(
            src_ref=route_out.at[other],
            dst_ref=route_in.at[c * count + k - 1],
            send_sem=send_sem.at[0],
            recv_sem=meta_sem.at[0],
            device_id=(other, core if c == 0 else 1 - core),
            device_id_type=MESH,
        ).start()

    scale = (NOPE + ROPE) ** (-0.5)
    pair = 2 * batch
    place = lax.broadcasted_iota(jnp.int32, (pair, length), 1)

    def twice(x):
        return jnp.concatenate([x, x], axis=0)

    def attend(b):
        whole(latent.at[b], cache_sem.at[0, b]).wait()
        whole(rope.at[b], cache_sem.at[1, b]).wait()
        if b == 0:
            for src, dst, i in stacked:
                pltpu.make_async_copy(src, dst, load_sem.at[i]).start()
        mine = query[b]
        row = lax.broadcasted_iota(jnp.int32, (tall, wide), 0) % batch
        spaced = jnp.concatenate(
            [jnp.where(row == j, mine, 0.0).astype(bf16) for j in range(batch)], axis=1
        )
        past = mul_t(latent[b], spaced)
        keys = rope[b].reshape(batch * ROPE, length)
        scores[...] = (past.T + mul(spun[b].astype(bf16), keys)) * scale
        at = slice(b * batch, (b + 1) * batch)
        own_key = twice(fresh[at])
        own_rope = twice(jnp.concatenate([new_rope[at]] * (batch * ROPE // 128), axis=1))
        limit = twice(lens[at])[:, :1].astype(jnp.int32)
        ends = []
        for i in range(HEADS // 2):
            span = slice(i * pair, (i + 1) * pair)
            own = jnp.sum(query[b, span] * own_key, axis=1, keepdims=True)
            own = (own + jnp.sum(spun[b, span] * own_rope, axis=1, keepdims=True)) * scale
            past = scores[span]
            valid = place < limit
            top = jnp.max(jnp.where(valid, past, -1e30), axis=1, keepdims=True)
            top = jnp.maximum(top, own)
            past = jnp.where(valid, jnp.exp(past - top), 0.0)
            own = jnp.exp(own - top)
            total = jnp.sum(past, axis=1, keepdims=True) + own
            probs[span] = past.astype(bf16)
            ends.append((own.astype(bf16).astype(f32), 1.0 / total))
        seen = jnp.zeros((tall, wide), f32)
        for j in range(batch):
            out = mul(probs[...], latent[b, :, j * wide : (j + 1) * wide])
            seen = jnp.where(row == j, out, seen)
        for i, (own, inverse) in enumerate(ends):
            span = slice(i * pair, (i + 1) * pair)
            mixed[b, span] = (seen[span] + own * own_key) * inverse

    for b in range(batches):
        attend(b)

    loads[8].wait()
    parts = []
    for h in range(0, HEADS, 2):
        at = slice(h * VDIM, (h + 2) * VDIM)
        both = jnp.concatenate(
            [mixed[b, (h + i) * batch : (h + i + 1) * batch] for i in range(2) for b in range(batches)],
            axis=0,
        )
        both = mul(both.astype(bf16), w_uv[:, at])
        parts.append(jnp.where(lane < VDIM, both[:seqs], both[seqs:]))
    head_out = jnp.concatenate(parts, axis=1).astype(bf16)
    loads[9].wait()
    wait_small(7, 8)
    first = (tokens + rms_scale(mul(head_out, w_o[...]), post_gain[...][None, :])).astype(bf16)
    moe_in = rms_scale(first, moe_gain[...][None, :]).astype(bf16)
    rows[0, 0] = moe_in

    def row_copy(hop, src, dst, h):
        cut = slice(None) if h is None else pl.ds(h * half_width, half_width)
        return pltpu.make_async_remote_copy(
            src_ref=rows.at[0, src, :, cut],
            dst_ref=rows.at[0, dst, :, cut],
            send_sem=send_sem.at[1],
            recv_sem=row_recv.at[dst],
            device_id=peer(hop),
            device_id_type=MESH,
        )

    def relay_copy(g, m):
        return pltpu.make_async_remote_copy(
            src_ref=rows.at[0, g * size + m],
            dst_ref=rows.at[1, g * size + m],
            send_sem=send_sem.at[2],
            recv_sem=relay_recv.at[g],
            device_id=sibling,
            device_id_type=MESH,
        )

    def sib_copy(g):
        return pltpu.make_async_remote_copy(
            src_ref=to_sib.at[pl.ds(g * size, size)],
            dst_ref=from_sib.at[pl.ds(g * size, size)],
            send_sem=send_sem.at[3],
            recv_sem=sib_recv.at[g],
            device_id=sibling,
            device_id_type=MESH,
        )

    bits = bits_of(size)
    joint = [m for m in range(1, size) if m != low_bit(m)]

    def home_copy(g, m, hop, h):
        cut = slice(None) if h is None else pl.ds(h * half_width, half_width)
        sem = 1 - min(m, 1)
        if m in joint:
            sem = 2 + 2 * joint.index(m) + h
        return pltpu.make_async_remote_copy(
            src_ref=to_home.at[g * size + m, :, cut],
            dst_ref=from_home.at[g * size + m, :, cut],
            send_sem=send_sem.at[4],
            recv_sem=home_recv.at[g, sem],
            device_id=peer(hop),
            device_id_type=MESH,
        )

    def spread_base(g):
        for bit in bits:
            row_copy(bit, g * size, g * size + bit, None).start()
        relay_copy(g, 0).start()

    def arrive_base(g):
        row_copy(1, 0, g * size, None).wait_recv()
        spread_base(g)

    def arrive(g, m):
        k = g * size + m
        row_copy(1, 0, k, None).wait_recv()
        for h in range(2):
            for bit in bits:
                if (bit > high_bit(m)) if h == 0 else (bit < low_bit(m)):
                    row_copy(bit, k, k + bit, h).start()
        relay_copy(g, m).start()

    for g in list(range(groups - 1, 0, -1)):
        row_copy(g * size, 0, g * size, None).start()
    spread_base(0)

    whole(s_in, load_sem.at[10]).wait()
    whole(s_down, load_sem.at[11]).wait()
    hidden = (jax.nn.silu(mul(moe_in, s_in[0])) * mul(moe_in, s_in[1])).astype(bf16)
    shared_out = mul(hidden, s_down[...])

    whole(e_in, load_sem.at[12]).wait()
    whole(e_down, load_sem.at[13]).wait()
    whole(d_in, load_sem.at[6]).wait()
    whole(d_down, load_sem.at[7]).wait()
    whole(route_in, meta_sem.at[0]).wait()
    wait_small(9, 10)
    gate_rows = jnp.broadcast_to(dense_vec[...][None, :], (seqs, width))

    def weight_of(c, k):
        flat = route_out[me] if c + k == 0 else route_in[c * count + k - 1]
        return upright(flat[:, :seqs])

    def compute(g):
        block = rows[:, g * size : (g + 1) * size].reshape(2 * size * seqs, width)
        weights = jnp.concatenate(
            [weight_of(c, g * size + m) for c in range(2) for m in range(size)], axis=0
        )
        gate = jax.nn.sigmoid(mul_t(block, gate_rows)[:, :1])
        act = (jax.nn.silu(mul(block, e_in[0])) * mul(block, e_in[1])).astype(bf16)
        routed = mul(act, e_down[...]).astype(bf16).astype(f32)
        act = (jax.nn.silu(mul(block, d_in[0])) * mul(block, d_in[1])).astype(bf16)
        part = routed * weights + mul(act, d_down[...]) * gate
        part = part.reshape(2, size, seqs, width)
        to_sib[g * size : (g + 1) * size] = part[1].astype(bf16)
        sib_copy(g).start()
        keep[g * size : (g + 1) * size] = part[0]

    def send_home(g, m, h):
        home_copy(g, m, high_bit(m) if h == 0 else low_bit(m), h).start()

    def cut_of(h):
        return slice(h * half_width, (h + 1) * half_width)

    def inward(m, h):
        return [b for b in bits if ((b > high_bit(m)) if h == 0 else (b < low_bit(m)))]

    def home(g):
        sib_copy(g).wait_recv()
        for m in reversed(range(1, size)):
            k = g * size + m
            for h in range(2):
                part = keep[k, :, cut_of(h)] + from_sib[k, :, cut_of(h)].astype(f32)
                if inward(m, h):
                    keep[k, :, cut_of(h)] = part
                else:
                    to_home[k, :, cut_of(h)] = part.astype(bf16)
                    send_home(g, m, h)
        keep[g * size] = keep[g * size] + from_sib[g * size].astype(f32)

    def pass_on(g):
        for m in reversed(range(1, size)):
            k = g * size + m
            for h in range(2):
                if inward(m, h):
                    part = keep[k, :, cut_of(h)]
                    for bit in inward(m, h):
                        home_copy(g, m + bit, 1, h).wait_recv()
                        part = part + from_home[k + bit, :, cut_of(h)].astype(f32)
                    to_home[k, :, cut_of(h)] = part.astype(bf16)
                    send_home(g, m, h)

    def plane_sum(g):
        part = keep[g * size]
        landed = from_home.at[pl.ds(g * size, len(bits))]
        whole(landed, home_recv.at[g, 0]).wait()
        for bit in bits:
            part = part + from_home[g * size + bit].astype(f32)
        return part

    def send_far(g):
        to_home[g * size] = plane_sum(g).astype(bf16)
        home_copy(g, 0, g * size, None).start()

    def wait_relays(g):
        whole(rows.at[1, pl.ds(g * size, size)], relay_recv.at[g]).wait()

    def early(g):
        for m in range(1, size):
            if m not in joint:
                arrive(g, m)

    def late(g):
        for m in joint:
            arrive(g, m)

    def turn(g):
        wait_relays(g)
        compute(g)

    early(0)
    order = list(range(groups - 1, 0, -1))
    for g in order:
        arrive_base(g)
    late(0)
    order = [0] + order
    for g in order[1:]:
        early(g)
        if g == order[1]:
            turn(0)
    for i, g in enumerate(order):
        if i > 0:
            late(g)
            home(order[i - 1])
            if i > 1:
                pass_on(order[i - 2])
            turn(g)
    home(order[-1])
    for i in range(max(0, len(order) - 2), len(order)):
        pass_on(order[i])
    for g in order:
        if g > 0:
            send_far(g)
    total = shared_out + plane_sum(0)
    for g in range(1, groups):
        home_copy(g, 0, 1, None).wait_recv()
        total = total + from_home[g * size].astype(f32)
    inverse = lax.rsqrt(jnp.mean(total * total, axis=-1, keepdims=True) + eps)
    out_ref[...] = (
        first.astype(f32) + total * inverse * out_gain[...][None, :].astype(f32)
    ).astype(bf16)

    whole(route_in, send_sem.at[0]).wait()
    whole(rows.at[0, pl.ds(1, count - 1)], send_sem.at[1]).wait()
    whole(rows.at[0], send_sem.at[2]).wait()
    whole(to_sib, send_sem.at[3]).wait()
    whole(to_home.at[pl.ds(1, count - 1)], send_sem.at[4]).wait()


def shards(
    tokens,
    lengths,
    cache_latent,
    cache_rope,
    attn_gain,
    w_dq,
    q_gain,
    w_q_nope,
    w_q_rope,
    w_dkv,
    kv_gain,
    w_krope,
    w_uk,
    w_uv,
    w_o,
    post_gain,
    moe_gain,
    routes,
    route_scores,
    expert_gate,
    expert_up,
    expert_down,
    shared_gate,
    shared_up,
    shared_down,
    dense_vec,
    dense_w_gate,
    dense_w_up,
    dense_w_down,
    out_gain,
):
    f32, bf16 = jnp.float32, jnp.bfloat16
    count = lax.axis_size("ep")
    groups = min(4, count)
    seqs, width = tokens.shape
    _, length, wide = cache_latent.shape
    batch = 128 // HEADS
    batches = seqs // batch
    small = [tokens, lengths, routes.T, route_scores.T, attn_gain, q_gain, kv_gain]
    small += [post_gain, moe_gain, dense_vec, out_gain]
    big = [w_dq, w_dkv, w_krope.T, w_q_nope, w_q_rope, w_uk, cache_latent, cache_rope, w_uv, w_o]
    big += [shared_gate, shared_up, shared_down, expert_gate, expert_up, dense_w_gate, dense_w_up]
    big += [expert_down, dense_w_down]
    room = [pltpu.VMEM(w.shape, w.dtype) for w in small + big[:10]]
    room[17] = pltpu.VMEM((batches, length, batch * wide), bf16)
    room[18] = pltpu.VMEM((batches, batch) + cache_rope.shape[1:], bf16)
    room += [
        pltpu.VMEM((2,) + shared_gate.shape, bf16),
        pltpu.VMEM(shared_down.shape, bf16),
        pltpu.VMEM((2,) + expert_gate.shape[1:], bf16),
        pltpu.VMEM(expert_down.shape[1:], bf16),
        pltpu.VMEM((2,) + dense_w_gate.shape, bf16),
        pltpu.VMEM(dense_w_down.shape, bf16),
    ]
    vmem = pl.BlockSpec(memory_space=pltpu.VMEM)
    dma = pltpu.SemaphoreType.DMA
    blocks = (count, seqs, width)
    tall = HEADS * batch
    experts = expert_gate.shape[0] * count
    joint = count // groups - (count // groups).bit_length()
    return pl.pallas_call(
        functools.partial(layer_kernel, count, groups),
        out_shape=(pltpu.VMEM((seqs, width), bf16), pltpu.VMEM((seqs, wide), bf16)),
        in_specs=[pl.BlockSpec(memory_space=pltpu.HBM)] * (len(small) + len(big)),
        out_specs=(vmem, vmem),
        scratch_shapes=room
        + [
            pltpu.VMEM((batches, tall, wide), f32),
            pltpu.VMEM((batches, tall, batch * ROPE), f32),
            pltpu.VMEM((tall, length), f32),
            pltpu.VMEM((tall, length), bf16),
            pltpu.VMEM((batches, tall, wide), f32),
            pltpu.VMEM((2,) + blocks, bf16),
            pltpu.VMEM((experts, 1, 128), f32),
            pltpu.VMEM((2 * count - 1, 1, 128), f32),
            pltpu.VMEM(blocks, f32),
            pltpu.VMEM(blocks, bf16),
            pltpu.VMEM(blocks, bf16),
            pltpu.VMEM(blocks, bf16),
            pltpu.VMEM(blocks, bf16),
            dma((len(small),)),
            dma((14,)),
            dma((2, batches)),
            dma((1,)),
            dma((5,)),
            dma((count,)),
            dma((groups,)),
            dma((groups,)),
            dma((groups, 2 + 2 * joint)),
        ],
        compiler_params=pltpu.CompilerParams(collective_id=0, has_side_effects=True),
        name="layer",
    )(*small, *big)


def solution(mesh):
    return jax.shard_map(
        shards,
        mesh=mesh,
        in_specs=(
            P(("ep", "tp"), None),
            P(("ep", "tp")),
            P(("ep", "tp"), None, None),
            P(("ep", "tp"), None, None),
            P(),
            P(),
            P(),
            P(),
            P(),
            P(),
            P(),
            P(),
            P(),
            P(),
            P(),
            P(),
            P(),
            P(("ep", "tp"), None),
            P(("ep", "tp"), None),
            P("ep", None, "tp"),
            P("ep", None, "tp"),
            P("ep", "tp", None),
            P(),
            P(),
            P(),
            P(),
            P(None, ("ep", "tp")),
            P(None, ("ep", "tp")),
            P(("ep", "tp"), None),
            P(),
        ),
        out_specs=(P(("ep", "tp"), None), P(("ep", "tp"), None)),
        check_vma=False,
    )
```

time: 53.7 us -> 43.5 us (0.81)
  Pallas kernels: 46.3 us -> 41.4 us
  local copies, waits for them, and re-layouts: 5.52 us -> 1.22 us
  other arithmetic: 0.87 us -> 0 us
    pallas_call x2 -> x1, Pallas kernels: 46.3 us -> 41.4 us  [shards(): pl.pallas_call(functools.partial(layer_kernel, count, groups), out_shape=...]
    unnamed x3 -> x2, local copies, waits for them, and re-layouts: 4.08 us -> 1.22 us
    another operation x4 -> x0, local copies, waits for them, and re-layouts: 1.44 us -> none  [the longest x2 0.73 us: attention(): cosine = jnp.tile(jnp.concatenate([cosine, cosine], axis=1), (1, HEADS))]
    convert_element_type x1 -> x0, other arithmetic: 0.66 us -> none  [angles(): angle = lengths.astype(jnp.float32)[:, None] * freqs[None, :]]
where the time goes in v1:
time: 43.5 us; the launch traced here: 43.3 us
  Pallas kernels  41.4 us (95%)
  local copies, waits for them, and re-layouts  1.22 us (3%)
  between operations  0.65 us (1%)
    pallas_call x1, Pallas kernels, shards(): pl.pallas_call(functools.partial(layer_kernel, count, groups), out_shape=...  41.4 us
    unnamed x2, local copies, waits for them, and re-layouts  1.22 us

profile of v1, /device:TPU:0, one launch (start us, length us, event | category | flops | bytes accessed | tf_op | source)
XLA Modules:
  0.0 43.3 jit_solution(3786373102829688471)
XLA Ops:
  0.6 41.4 %layer.1 = (bf16[16,1024]{1,0:T(8,128)(2,1)S(1)}, bf16[16,256]{1,0:T(8,128)(2,1)S(1)}) custom-call(bf16[16,1024]{1,0:T(8,128)(2,1)} %refs_0_.1, s32[16]{0:T(128)} %refs_1_.1, s32[4,16]{1,0:T(4,128)} %bitcast.4, f32[4,16]{1,0:T(4,128)} %bitcast.5, bf16[1024]{0:T(1024)(128)(2,1)} %refs_4_.1, bf16[512]{0:T(512)(128)(2,1)} %refs_5_.1, bf16[256]{0:T(256)(128)(2,1)} %refs_6_.1, ...), custom_call_target="tpu_custom_call" | custom-call | tf_op jit(solution)/shard_map/layer/pallas_call | solution.py:569
  42.1 0.6 %copy.34 = bf16[16,1024]{1,0:T(8,128)(2,1)} copy(bf16[16,1024]{1,0:T(8,128)(2,1)S(1)} %get-tuple-element.2) | data formatting | bytes 65536
  42.7 0.6 %copy.35 = bf16[16,256]{1,0:T(8,128)(2,1)} copy(bf16[16,256]{1,0:T(8,128)(2,1)S(1)} %get-tuple-element.3) | data formatting | bytes 16384

commit v2 on v1

--- a/solution.py
+++ b/solution.py
@@ -25,27 +25,6 @@
 
 
 MESH = pl.DeviceIdType.MESH
-
-
-def partner(me, k, count):
-    other, bit = me, 1
-    while bit < count:
-        if (k // bit) % 2:
-            other = other + bit * (1 - 2 * ((me // bit) % 2))
-        bit *= 2
-    return other
-
-
-def bits_of(size):
-    return [1 << i for i in range(size.bit_length() - 1)]
-
-
-def low_bit(m):
-    return m & -m
-
-
-def high_bit(m):
-    return 1 << (m.bit_length() - 1)
 
 
 def layer_kernel(
@@ -57,9 +36,9 @@
     small, hbm, (out_ref, latent_out) = refs[:11], refs[11:30], refs[30:32]
     smalls, bufs = refs[32:43], refs[43:59]
     (query, spun, scores, probs, mixed, rows, route_out, route_in) = refs[59:67]
-    (keep, to_sib, from_sib, to_home, from_home) = refs[67:72]
-    (small_sem, load_sem, cache_sem, meta_sem, send_sem, row_recv, relay_recv) = refs[72:79]
-    sib_recv, home_recv = refs[79:]
+    (keep, to_home, from_home) = refs[67:70]
+    (small_sem, load_sem, cache_sem, twin_sem, meta_sem, send_sem) = refs[70:76]
+    row_recv, near_recv, plane_recv, far_recv = refs[76:]
     (tokens_ref, lens_ref, routes_ref, scores_ref, attn_gain, q_gain, kv_gain) = smalls[:7]
     post_gain, moe_gain, dense_vec, out_gain = smalls[7:]
     w_dq, w_dkv, w_krope, w_q_nope, w_q_rope, w_uk, latent, rope, w_uv, w_o = bufs[:10]
@@ -70,13 +49,19 @@
     wide = spread // batch
     tall = HEADS * batch
     size = count // groups
-    half_width = width // 2
     me = lax.axis_index("ep")
     core = lax.axis_index("tp")
-    sibling = (me, 1 - core)
+    flips = {bit: bit * (1 - 2 * ((me // bit) % 2)) for bit in (1 << i for i in range(count.bit_length() - 1))}
+
+    def partner(k):
+        other = me
+        for bit in flips:
+            if k & bit:
+                other = other + flips[bit]
+        return other
 
     def peer(k):
-        return (partner(me, k, count), core)
+        return (partner(k), core)
 
     small_loads = [
         pltpu.make_async_copy(src, dst, small_sem.at[i])
@@ -97,12 +82,12 @@
         (hbm[10], s_in.at[0], 10),
         (hbm[11], s_in.at[1], 10),
         (hbm[12], s_down, 11),
-        (hbm[13].at[0], e_in.at[0], 12),
-        (hbm[14].at[0], e_in.at[1], 12),
-        (hbm[17].at[0], e_down, 13),
-        (hbm[15], d_in.at[0], 6),
-        (hbm[16], d_in.at[1], 6),
-        (hbm[18], d_down, 7),
+        (hbm[13].at[0], e_in.at[0, 0], 12),
+        (hbm[14].at[0], e_in.at[0, 1], 12),
+        (hbm[17].at[0], e_down.at[0], 13),
+        (hbm[15], d_in.at[0, 0], 6),
+        (hbm[16], d_in.at[0, 1], 6),
+        (hbm[18], d_down.at[0], 7),
     ]
 
     def whole(ref, sem):
@@ -119,11 +104,9 @@
         loads[i].start()
 
     barrier = pltpu.get_barrier_semaphore()
-    pl.semaphore_signal(barrier, inc=1, device_id=sibling, device_id_type=MESH)
+    pl.semaphore_signal(barrier, inc=1, device_id=(me, 1 - core), device_id_type=MESH)
     for k in range(1, count):
-        other = partner(me, k, count)
-        for c in (core, 1 - core):
-            pl.semaphore_signal(barrier, inc=1, device_id=(other, c), device_id_type=MESH)
+        pl.semaphore_signal(barrier, inc=1, device_id=peer(k), device_id_type=MESH)
 
     def mul(a, b):
         return jnp.dot(a, b, preferred_element_type=f32)
@@ -221,17 +204,29 @@
                     i * seqs + b * batch : i * seqs + (b + 1) * batch
                 ]
 
-    pl.semaphore_wait(barrier, 2 * count - 1)
-
-    others = [(c, k) for c in range(2) for k in range(count) if c + k > 0]
-    for c, k in others:
-        other = partner(me, k, count)
+    pl.semaphore_wait(barrier, count)
+
+    twin = ((e_in, 0), (e_down, 1), (d_in, 2), (d_down, 3))
+    into = {13: e_in.at[1, 0], 14: e_in.at[1, 1], 17: e_down.at[1]}
+    into.update({15: d_in.at[1, 0], 16: d_in.at[1, 1], 18: d_down.at[1]})
+    for i, sem in ((13, 0), (14, 0), (17, 1), (15, 2), (16, 2), (18, 3)):
+        pltpu.make_async_remote_copy(
+            src_ref=hbm[i].at[0] if len(hbm[i].shape) == 3 else hbm[i],
+            dst_ref=into[i],
+            send_sem=twin_sem.at[0, sem],
+            recv_sem=twin_sem.at[1, sem],
+            device_id=(me, 1 - core),
+            device_id_type=MESH,
+        ).start()
+
+    for k in range(1, count):
+        other = partner(k)
         pltpu.make_async_remote_copy(
             src_ref=route_out.at[other],
-            dst_ref=route_in.at[c * count + k - 1],
+            dst_ref=route_in.at[k - 1],
             send_sem=send_sem.at[0],
             recv_sem=meta_sem.at[0],
-            device_id=(other, core if c == 0 else 1 - core),
+            device_id=(other, core),
             device_id_type=MESH,
         ).start()
 
@@ -253,9 +248,12 @@
         spaced = jnp.concatenate(
             [jnp.where(row == j, mine, 0.0).astype(bf16) for j in range(batch)], axis=1
         )
-        past = mul_t(latent[b], spaced)
         keys = rope[b].reshape(batch * ROPE, length)
-        scores[...] = (past.T + mul(spun[b].astype(bf16), keys)) * scale
+        turned = spun[b].astype(bf16)
+        for r in range(2):
+            cut = slice(r * (length // 2), (r + 1) * (length // 2))
+            past = mul_t(latent[b, cut], spaced)
+            scores[:, cut] = (past.T + mul(turned, keys[:, cut])) * scale
         at = slice(b * batch, (b + 1) * batch)
         own_key = twice(fresh[at])
         own_rope = twice(jnp.concatenate([new_rope[at]] * (batch * ROPE // 128), axis=1))
@@ -300,209 +298,148 @@
     wait_small(7, 8)
     first = (tokens + rms_scale(mul(head_out, w_o[...]), post_gain[...][None, :])).astype(bf16)
     moe_in = rms_scale(first, moe_gain[...][None, :]).astype(bf16)
-    rows[0, 0] = moe_in
-
-    def row_copy(hop, src, dst, h):
-        cut = slice(None) if h is None else pl.ds(h * half_width, half_width)
+    rows[0] = moe_in
+
+    def row_copy(hop, src, dst):
         return pltpu.make_async_remote_copy(
-            src_ref=rows.at[0, src, :, cut],
-            dst_ref=rows.at[0, dst, :, cut],
+            src_ref=rows.at[src],
+            dst_ref=rows.at[dst],
             send_sem=send_sem.at[1],
             recv_sem=row_recv.at[dst],
             device_id=peer(hop),
             device_id_type=MESH,
         )
 
-    def relay_copy(g, m):
+    def home_copy(k, hop, recv_sem):
         return pltpu.make_async_remote_copy(
-            src_ref=rows.at[0, g * size + m],
-            dst_ref=rows.at[1, g * size + m],
+            src_ref=to_home.at[k],
+            dst_ref=from_home.at[k],
             send_sem=send_sem.at[2],
-            recv_sem=relay_recv.at[g],
-            device_id=sibling,
-            device_id_type=MESH,
-        )
-
-    def sib_copy(g):
-        return pltpu.make_async_remote_copy(
-            src_ref=to_sib.at[pl.ds(g * size, size)],
-            dst_ref=from_sib.at[pl.ds(g * size, size)],
-            send_sem=send_sem.at[3],
-            recv_sem=sib_recv.at[g],
-            device_id=sibling,
-            device_id_type=MESH,
-        )
-
-    bits = bits_of(size)
-    joint = [m for m in range(1, size) if m != low_bit(m)]
-
-    def home_copy(g, m, hop, h):
-        cut = slice(None) if h is None else pl.ds(h * half_width, half_width)
-        sem = 1 - min(m, 1)
-        if m in joint:
-            sem = 2 + 2 * joint.index(m) + h
-        return pltpu.make_async_remote_copy(
-            src_ref=to_home.at[g * size + m, :, cut],
-            dst_ref=from_home.at[g * size + m, :, cut],
-            send_sem=send_sem.at[4],
-            recv_sem=home_recv.at[g, sem],
+            recv_sem=recv_sem,
             device_id=peer(hop),
             device_id_type=MESH,
         )
 
-    def spread_base(g):
-        for bit in bits:
-            row_copy(bit, g * size, g * size + bit, None).start()
-        relay_copy(g, 0).start()
-
-    def arrive_base(g):
-        row_copy(1, 0, g * size, None).wait_recv()
-        spread_base(g)
-
-    def arrive(g, m):
-        k = g * size + m
-        row_copy(1, 0, k, None).wait_recv()
-        for h in range(2):
-            for bit in bits:
-                if (bit > high_bit(m)) if h == 0 else (bit < low_bit(m)):
-                    row_copy(bit, k, k + bit, h).start()
-        relay_copy(g, m).start()
-
-    for g in list(range(groups - 1, 0, -1)):
-        row_copy(g * size, 0, g * size, None).start()
-    spread_base(0)
-
+    near = [1] if groups > 1 else []
+    far = list(range(groups - 1, 1, -1))
+    single = [m for m in range(1, size) if m & (m - 1) == 0]
+    joint = [m for m in range(1, size) if m & (m - 1)]
+
+    def spread_base(g, ms):
+        for m in ms:
+            row_copy(m, g * size, g * size + m).start()
+
+    def arrive(k):
+        row_copy(1, 0, k).wait_recv()
+
+    for g in far + near:
+        row_copy(g * size, 0, g * size).start()
+    spread_base(0, single + joint)
     whole(s_in, load_sem.at[10]).wait()
     whole(s_down, load_sem.at[11]).wait()
     hidden = (jax.nn.silu(mul(moe_in, s_in[0])) * mul(moe_in, s_in[1])).astype(bf16)
     shared_out = mul(hidden, s_down[...])
 
-    whole(e_in, load_sem.at[12]).wait()
-    whole(e_down, load_sem.at[13]).wait()
-    whole(d_in, load_sem.at[6]).wait()
-    whole(d_down, load_sem.at[7]).wait()
-    whole(route_in, meta_sem.at[0]).wait()
     wait_small(9, 10)
     gate_rows = jnp.broadcast_to(dense_vec[...][None, :], (seqs, width))
 
-    def weight_of(c, k):
-        flat = route_out[me] if c + k == 0 else route_in[c * count + k - 1]
+    def wait_weights():
+        for ref, sem in ((e_in, 12), (e_down, 13), (d_in, 6), (d_down, 7)):
+            whole(ref.at[0], load_sem.at[sem]).wait()
+        for ref, sem in twin:
+            whole(ref.at[1], twin_sem.at[1, sem]).wait()
+        whole(route_in, meta_sem.at[0]).wait()
+
+    def weight_of(k):
+        flat = route_out[me] if k == 0 else route_in[k - 1]
         return upright(flat[:, :seqs])
 
-    def compute(g):
-        block = rows[:, g * size : (g + 1) * size].reshape(2 * size * seqs, width)
-        weights = jnp.concatenate(
-            [weight_of(c, g * size + m) for c in range(2) for m in range(size)], axis=0
-        )
+    def compute(start, stop):
+        lo, hi = start * size, stop * size
+        block = rows[lo:hi].reshape((hi - lo) * seqs, width)
+        weights = jnp.concatenate([weight_of(k) for k in range(lo, hi)], axis=0)
         gate = jax.nn.sigmoid(mul_t(block, gate_rows)[:, :1])
-        act = (jax.nn.silu(mul(block, e_in[0])) * mul(block, e_in[1])).astype(bf16)
-        routed = mul(act, e_down[...]).astype(bf16).astype(f32)
-        act = (jax.nn.silu(mul(block, d_in[0])) * mul(block, d_in[1])).astype(bf16)
-        part = routed * weights + mul(act, d_down[...]) * gate
-        part = part.reshape(2, size, seqs, width)
-        to_sib[g * size : (g + 1) * size] = part[1].astype(bf16)
-        sib_copy(g).start()
-        keep[g * size : (g + 1) * size] = part[0]
-
-    def send_home(g, m, h):
-        home_copy(g, m, high_bit(m) if h == 0 else low_bit(m), h).start()
-
-    def cut_of(h):
-        return slice(h * half_width, (h + 1) * half_width)
-
-    def inward(m, h):
-        return [b for b in bits if ((b > high_bit(m)) if h == 0 else (b < low_bit(m)))]
-
-    def home(g):
-        sib_copy(g).wait_recv()
-        for m in reversed(range(1, size)):
-            k = g * size + m
-            for h in range(2):
-                part = keep[k, :, cut_of(h)] + from_sib[k, :, cut_of(h)].astype(f32)
-                if inward(m, h):
-                    keep[k, :, cut_of(h)] = part
-                else:
-                    to_home[k, :, cut_of(h)] = part.astype(bf16)
-                    send_home(g, m, h)
-        keep[g * size] = keep[g * size] + from_sib[g * size].astype(f32)
-
-    def pass_on(g):
-        for m in reversed(range(1, size)):
-            k = g * size + m
-            for h in range(2):
-                if inward(m, h):
-                    part = keep[k, :, cut_of(h)]
-                    for bit in inward(m, h):
-                        home_copy(g, m + bit, 1, h).wait_recv()
-                        part = part + from_home[k + bit, :, cut_of(h)].astype(f32)
-                    to_home[k, :, cut_of(h)] = part.astype(bf16)
-                    send_home(g, m, h)
+        pairs = [(ref[c], down[c]) for ref, down in ((e_in, e_down), (d_in, d_down)) for c in range(2)]
+        opened = [(mul(block, pair[0]), mul(block, pair[1])) for pair, _ in pairs]
+        acts = [(jax.nn.silu(x) * y).astype(bf16) for x, y in opened]
+        outs = [mul(x, down) for x, (_, down) in zip(acts, pairs)]
+        routed = sum(x.astype(bf16).astype(f32) for x in outs[:2])
+        part = routed * weights + (outs[2] + outs[3]) * gate
+        keep[lo:hi] = part.reshape(hi - lo, seqs, width)
+
+    def home_near():
+        for m in range(size - 1, -1, -1):
+            to_home[size + m] = keep[size + m].astype(bf16)
+            home_copy(size + m, size, near_recv.at[m]).start()
+
+    def gather_near():
+        for m in range(size - 1, -1, -1):
+            home_copy(size + m, 1, near_recv.at[m]).wait_recv()
+            keep[m] = keep[m] + from_home[size + m].astype(f32)
+
+    def home(g, ms):
+        for m in ms:
+            to_home[g * size + m] = keep[g * size + m].astype(bf16)
+            home_copy(g * size + m, m, plane_recv.at[g]).start()
 
     def plane_sum(g):
         part = keep[g * size]
-        landed = from_home.at[pl.ds(g * size, len(bits))]
-        whole(landed, home_recv.at[g, 0]).wait()
-        for bit in bits:
-            part = part + from_home[g * size + bit].astype(f32)
+        if size > 1:
+            whole(from_home.at[pl.ds(g * size + 1, size - 1)], plane_recv.at[g]).wait()
+        for m in range(1, size):
+            part = part + from_home[g * size + m].astype(f32)
         return part
 
     def send_far(g):
         to_home[g * size] = plane_sum(g).astype(bf16)
-        home_copy(g, 0, g * size, None).start()
-
-    def wait_relays(g):
-        whole(rows.at[1, pl.ds(g * size, size)], relay_recv.at[g]).wait()
-
-    def early(g):
-        for m in range(1, size):
-            if m not in joint:
-                arrive(g, m)
-
-    def late(g):
-        for m in joint:
-            arrive(g, m)
-
-    def turn(g):
-        wait_relays(g)
-        compute(g)
-
-    early(0)
-    order = list(range(groups - 1, 0, -1))
-    for g in order:
-        arrive_base(g)
-    late(0)
-    order = [0] + order
-    for g in order[1:]:
-        early(g)
-        if g == order[1]:
-            turn(0)
-    for i, g in enumerate(order):
-        if i > 0:
-            late(g)
-            home(order[i - 1])
-            if i > 1:
-                pass_on(order[i - 2])
-            turn(g)
-    home(order[-1])
-    for i in range(max(0, len(order) - 2), len(order)):
-        pass_on(order[i])
-    for g in order:
-        if g > 0:
-            send_far(g)
+        home_copy(g * size, g * size, far_recv.at[g]).start()
+
+    for m in single:
+        arrive(m)
+        for g in near:
+            row_copy(size, m, size + m).start()
+    for g in far:
+        arrive(g * size)
+        spread_base(g, single)
+    for g in far:
+        spread_base(g, joint)
+    for m in joint:
+        arrive(m)
+        for g in near:
+            row_copy(size, m, size + m).start()
+    wait_weights()
+    compute(0, 1)
+    if near:
+        for m in range(size):
+            arrive(size + m)
+        compute(1, 2)
+        home_near()
+    if far:
+        for k in range(2 * size, count):
+            if k % size:
+                arrive(k)
+        compute(2, groups)
+        for g in far:
+            home(g, joint + single)
+    if near:
+        gather_near()
+    home(0, joint + single)
+    for g in far:
+        send_far(g)
     total = shared_out + plane_sum(0)
-    for g in range(1, groups):
-        home_copy(g, 0, 1, None).wait_recv()
+    for g in far:
+        home_copy(g * size, 1, far_recv.at[g]).wait_recv()
         total = total + from_home[g * size].astype(f32)
     inverse = lax.rsqrt(jnp.mean(total * total, axis=-1, keepdims=True) + eps)
     out_ref[...] = (
         first.astype(f32) + total * inverse * out_gain[...][None, :].astype(f32)
     ).astype(bf16)
 
+    for ref, sem in twin:
+        whole(ref.at[1], twin_sem.at[0, sem]).wait()
     whole(route_in, send_sem.at[0]).wait()
-    whole(rows.at[0, pl.ds(1, count - 1)], send_sem.at[1]).wait()
-    whole(rows.at[0], send_sem.at[2]).wait()
-    whole(to_sib, send_sem.at[3]).wait()
-    whole(to_home.at[pl.ds(1, count - 1)], send_sem.at[4]).wait()
+    whole(rows.at[pl.ds(1, count - 1)], send_sem.at[1]).wait()
+    whole(to_home.at[pl.ds(1, count - 1)], send_sem.at[2]).wait()
 
 
 def shards(
@@ -555,17 +492,16 @@
     room += [
         pltpu.VMEM((2,) + shared_gate.shape, bf16),
         pltpu.VMEM(shared_down.shape, bf16),
-        pltpu.VMEM((2,) + expert_gate.shape[1:], bf16),
-        pltpu.VMEM(expert_down.shape[1:], bf16),
-        pltpu.VMEM((2,) + dense_w_gate.shape, bf16),
-        pltpu.VMEM(dense_w_down.shape, bf16),
+        pltpu.VMEM((2, 2) + expert_gate.shape[1:], bf16),
+        pltpu.VMEM((2,) + expert_down.shape[1:], bf16),
+        pltpu.VMEM((2, 2) + dense_w_gate.shape, bf16),
+        pltpu.VMEM((2,) + dense_w_down.shape, bf16),
     ]
     vmem = pl.BlockSpec(memory_space=pltpu.VMEM)
     dma = pltpu.SemaphoreType.DMA
     blocks = (count, seqs, width)
     tall = HEADS * batch
     experts = expert_gate.shape[0] * count
-    joint = count // groups - (count // groups).bit_length()
     return pl.pallas_call(
         functools.partial(layer_kernel, count, groups),
         out_shape=(pltpu.VMEM((seqs, width), bf16), pltpu.VMEM((seqs, wide), bf16)),
@@ -578,23 +514,22 @@
             pltpu.VMEM((tall, length), f32),
             pltpu.VMEM((tall, length), bf16),
             pltpu.VMEM((batches, tall, wide), f32),
-            pltpu.VMEM((2,) + blocks, bf16),
+            pltpu.VMEM(blocks, bf16),
             pltpu.VMEM((experts, 1, 128), f32),
-            pltpu.VMEM((2 * count - 1, 1, 128), f32),
+            pltpu.VMEM((count - 1, 1, 128), f32),
             pltpu.VMEM(blocks, f32),
-            pltpu.VMEM(blocks, bf16),
-            pltpu.VMEM(blocks, bf16),
             pltpu.VMEM(blocks, bf16),
             pltpu.VMEM(blocks, bf16),
             dma((len(small),)),
             dma((14,)),
             dma((2, batches)),
+            dma((2, 4)),
             dma((1,)),
-            dma((5,)),
+            dma((3,)),
             dma((count,)),
+            dma((count // groups,)),
             dma((groups,)),
             dma((groups,)),
-            dma((groups, 2 + 2 * joint)),
         ],
         compiler_params=pltpu.CompilerParams(collective_id=0, has_side_effects=True),
         name="layer",

time: 43.5 us -> 33.2 us (0.76)
  Pallas kernels: 41.4 us -> 31.2 us
    pallas_call x1, Pallas kernels: 41.4 us -> 31.2 us  [shards(): pl.pallas_call(functools.partial(layer_kernel, count, groups), out_shape=...]
where the time goes in v2:
time: 33.2 us; the launch traced here: 33.1 us
  Pallas kernels  31.2 us (94%)
  local copies, waits for them, and re-layouts  1.22 us (4%)
  between operations  0.65 us (2%)
    pallas_call x1, Pallas kernels, shards(): pl.pallas_call(functools.partial(layer_kernel, count, groups), out_shape=...  31.2 us
    unnamed x2, local copies, waits for them, and re-layouts  1.22 us

profile of v2, /device:TPU:0, one launch (start us, length us, event | category | flops | bytes accessed | tf_op | source)
XLA Modules:
  0.0 33.1 jit_solution(14653089677412042129)
XLA Ops:
  0.6 31.2 %layer.1 = (bf16[16,1024]{1,0:T(8,128)(2,1)S(1)}, bf16[16,256]{1,0:T(8,128)(2,1)S(1)}) custom-call(bf16[16,1024]{1,0:T(8,128)(2,1)} %refs_0_.1, s32[16]{0:T(128)} %refs_1_.1, s32[4,16]{1,0:T(4,128)} %bitcast.4, f32[4,16]{1,0:T(4,128)} %bitcast.5, bf16[1024]{0:T(1024)(128)(2,1)} %refs_4_.1, bf16[512]{0:T(512)(128)(2,1)} %refs_5_.1, bf16[256]{0:T(256)(128)(2,1)} %refs_6_.1, ...), custom_call_target="tpu_custom_call" | custom-call | tf_op jit(solution)/shard_map/layer/pallas_call | solution.py:505
  31.9 0.6 %copy.34 = bf16[16,1024]{1,0:T(8,128)(2,1)} copy(bf16[16,1024]{1,0:T(8,128)(2,1)S(1)} %get-tuple-element.2) | data formatting | bytes 65536
  32.5 0.6 %copy.35 = bf16[16,256]{1,0:T(8,128)(2,1)} copy(bf16[16,256]{1,0:T(8,128)(2,1)S(1)} %get-tuple-element.3) | data formatting | bytes 16384

commit v3 on v2

--- a/solution.py
+++ b/solution.py
@@ -96,9 +96,13 @@
     def load_cache(b):
         for j in range(batch):
             s = b * batch + j
-            dst = latent.at[b, :, pl.ds(j * wide, wide)]
-            pltpu.make_async_copy(hbm[6].at[s], dst, cache_sem.at[0, b]).start()
-            pltpu.make_async_copy(hbm[7].at[s], rope.at[b, j], cache_sem.at[1, b]).start()
+            pltpu.make_async_copy(hbm[7].at[s], rope.at[b, j], cache_sem.at[2, b]).start()
+        for r in range(2):
+            cut = pl.ds(r * (length // 2), length // 2)
+            for j in range(batch):
+                src = hbm[6].at[b * batch + j, cut]
+                dst = latent.at[b, cut, pl.ds(j * wide, wide)]
+                pltpu.make_async_copy(src, dst, cache_sem.at[r, b]).start()
 
     for i in range(3):
         loads[i].start()
@@ -160,16 +164,14 @@
     loads[0].wait()
     load_cache(0)
     q_normed = rms_scale(mul(normed, w_dq[...]), q_gain[...][None, :]).astype(bf16)
-    loads[1].wait()
+    for i in range(1, 6):
+        loads[i].wait()
     new_latent = rms_scale(mul(normed, w_dkv[...]), kv_gain[...][None, :]).astype(bf16)
     latent_out[...] = new_latent
     fresh = new_latent.astype(f32)
-    loads[2].wait()
     raw = mul_t(normed, w_krope[...])
     new_rope = spin(jnp.concatenate([raw] * (128 // ROPE), axis=1))
-    loads[3].wait()
     q_nope = mul(q_normed, w_q_nope[...]).astype(bf16)
-    loads[4].wait()
     raw = mul(q_normed, w_q_rope[...])
     per = 128 // ROPE
     for a in range(HEADS // per):
@@ -186,11 +188,6 @@
                     spun[b, h * batch : (h + 1) * batch, v * 128 : (v + 1) * 128] = jnp.where(
                         (line % batch) // per == v, pick, 0.0
                     )[b * batch : (b + 1) * batch]
-    loads[5].wait()
-    for i in range(1, batches):
-        load_cache(i)
-    loads[8].start()
-    loads[9].start()
     low = lax.broadcasted_iota(jnp.int32, (seqs, 2 * NOPE), 1) < NOPE
     for pair in range(HEADS // 2):
         at = slice(pair * 2 * NOPE, (pair + 1) * 2 * NOPE)
@@ -206,6 +203,10 @@
 
     pl.semaphore_wait(barrier, count)
 
+    for i in range(1, batches):
+        load_cache(i)
+    loads[8].start()
+    loads[9].start()
     twin = ((e_in, 0), (e_down, 1), (d_in, 2), (d_down, 3))
     into = {13: e_in.at[1, 0], 14: e_in.at[1, 1], 17: e_down.at[1]}
     into.update({15: d_in.at[1, 0], 16: d_in.at[1, 1], 18: d_down.at[1]})
@@ -238,22 +239,33 @@
         return jnp.concatenate([x, x], axis=0)
 
     def attend(b):
-        whole(latent.at[b], cache_sem.at[0, b]).wait()
-        whole(rope.at[b], cache_sem.at[1, b]).wait()
-        if b == 0:
-            for src, dst, i in stacked:
-                pltpu.make_async_copy(src, dst, load_sem.at[i]).start()
+        if b > 0:
+            for r in range(2):
+                half_cut = slice(r * (length // 2), (r + 1) * (length // 2))
+                whole(latent.at[b, half_cut], cache_sem.at[r, b]).wait()
+            whole(rope.at[b], cache_sem.at[2, b]).wait()
         mine = query[b]
         row = lax.broadcasted_iota(jnp.int32, (tall, wide), 0) % batch
         spaced = jnp.concatenate(
             [jnp.where(row == j, mine, 0.0).astype(bf16) for j in range(batch)], axis=1
         )
-        keys = rope[b].reshape(batch * ROPE, length)
         turned = spun[b].astype(bf16)
         for r in range(2):
-            cut = slice(r * (length // 2), (r + 1) * (length // 2))
-            past = mul_t(latent[b, cut], spaced)
-            scores[:, cut] = (past.T + mul(turned, keys[:, cut])) * scale
+            half_cut = slice(r * (length // 2), (r + 1) * (length // 2))
+            if b == 0:
+                whole(latent.at[b, half_cut], cache_sem.at[r, b]).wait()
+            if b == 0 and r == 0:
+                whole(rope.at[b], cache_sem.at[2, b]).wait()
+            parts = 2 if b == 0 else 1
+            for i in range(parts):
+                long = length // 2 // parts
+                cut = slice((parts * r + i) * long, (parts * r + i + 1) * long)
+                past = mul_t(latent[b, cut], spaced)
+                turning = mul(turned, rope[b].reshape(batch * ROPE, length)[:, cut])
+                scores[:, cut] = (past.T + turning) * scale
+        if b == 0:
+            for src, dst, i in stacked:
+                pltpu.make_async_copy(src, dst, load_sem.at[i]).start()
         at = slice(b * batch, (b + 1) * batch)
         own_key = twice(fresh[at])
         own_rope = twice(jnp.concatenate([new_rope[at]] * (batch * ROPE // 128), axis=1))
@@ -368,14 +380,21 @@
         keep[lo:hi] = part.reshape(hi - lo, seqs, width)
 
     def home_near():
-        for m in range(size - 1, -1, -1):
+        for m in joint + single + [0]:
             to_home[size + m] = keep[size + m].astype(bf16)
             home_copy(size + m, size, near_recv.at[m]).start()
 
-    def gather_near():
-        for m in range(size - 1, -1, -1):
-            home_copy(size + m, 1, near_recv.at[m]).wait_recv()
-            keep[m] = keep[m] + from_home[size + m].astype(f32)
+    def gather_near(ms):
+        for m in ms:
+            part = keep[m]
+            if near:
+                home_copy(size + m, 1, near_recv.at[m]).wait_recv()
+                part = part + from_home[size + m].astype(f32)
+            if m > 0:
+                to_home[m] = part.astype(bf16)
+                home_copy(m, m, plane_recv.at[0]).start()
+            else:
+                keep[0] = part
 
     def home(g, ms):
         for m in ms:
@@ -400,32 +419,34 @@
             row_copy(size, m, size + m).start()
     for g in far:
         arrive(g * size)
-        spread_base(g, single)
-    for g in far:
-        spread_base(g, joint)
+        spread_base(g, joint + single)
     for m in joint:
         arrive(m)
         for g in near:
             row_copy(size, m, size + m).start()
     wait_weights()
     compute(0, 1)
+    def far_turn(g):
+        for m in range(1, size):
+            arrive(g * size + m)
+        compute(g, g + 1)
+        home(g, joint + single)
+
+    for g in far[:1]:
+        far_turn(g)
     if near:
         for m in range(size):
             arrive(size + m)
         compute(1, 2)
         home_near()
-    if far:
-        for k in range(2 * size, count):
-            if k % size:
-                arrive(k)
-        compute(2, groups)
-        for g in far:
-            home(g, joint + single)
-    if near:
-        gather_near()
-    home(0, joint + single)
-    for g in far:
+    for g in far[1:]:
+        far_turn(g)
+    for g in far[:1]:
         send_far(g)
+    gather_near(joint + single)
+    for g in far[1:]:
+        send_far(g)
+    gather_near([0])
     total = shared_out + plane_sum(0)
     for g in far:
         home_copy(g * size, 1, far_recv.at[g]).wait_recv()
@@ -522,7 +543,7 @@
             pltpu.VMEM(blocks, bf16),
             dma((len(small),)),
             dma((14,)),
-            dma((2, batches)),
+            dma((3, batches)),
             dma((2, 4)),
             dma((1,)),
             dma((3,)),

time: 33.2 us -> 31.7 us (0.955)
  Pallas kernels: 31.2 us -> 29.7 us
    pallas_call x1, Pallas kernels: 31.2 us -> 29.7 us  [shards(): pl.pallas_call(functools.partial(layer_kernel, count, groups), out_shape=...]
where the time goes in v3:
time: 31.7 us; the launch traced here: 31.6 us
  Pallas kernels  29.7 us (94%)
  local copies, waits for them, and re-layouts  1.22 us (4%)
  between operations  0.65 us (2%)
    pallas_call x1, Pallas kernels, shards(): pl.pallas_call(functools.partial(layer_kernel, count, groups), out_shape=...  29.7 us
    unnamed x2, local copies, waits for them, and re-layouts  1.22 us

profile of v3, /device:TPU:0, one launch (start us, length us, event | category | flops | bytes accessed | tf_op | source)
XLA Modules:
  0.0 31.6 jit_solution(12147101360013218150)
XLA Ops:
  0.6 29.7 %layer.1 = (bf16[16,1024]{1,0:T(8,128)(2,1)S(1)}, bf16[16,256]{1,0:T(8,128)(2,1)S(1)}) custom-call(bf16[16,1024]{1,0:T(8,128)(2,1)} %refs_0_.1, s32[16]{0:T(128)} %refs_1_.1, s32[4,16]{1,0:T(4,128)} %bitcast.4, f32[4,16]{1,0:T(4,128)} %bitcast.5, bf16[1024]{0:T(1024)(128)(2,1)} %refs_4_.1, bf16[512]{0:T(512)(128)(2,1)} %refs_5_.1, bf16[256]{0:T(256)(128)(2,1)} %refs_6_.1, ...), custom_call_target="tpu_custom_call" | custom-call | tf_op jit(solution)/shard_map/layer/pallas_call | solution.py:526
  30.4 0.6 %copy.34 = bf16[16,1024]{1,0:T(8,128)(2,1)} copy(bf16[16,1024]{1,0:T(8,128)(2,1)S(1)} %get-tuple-element.2) | data formatting | bytes 65536
  31.0 0.6 %copy.35 = bf16[16,256]{1,0:T(8,128)(2,1)} copy(bf16[16,256]{1,0:T(8,128)(2,1)S(1)} %get-tuple-element.3) | data formatting | bytes 16384
